TPU v7x, 32 devices: a whole 2x2x4 slice. The times are simulated.
32 devices in a mesh: grp: 2 (over y), sp: 4 (over z), tp: 4 (over x, core).
Axes of the slice: x: 2, y: 2, z: 4, core: 2. Of those that a mesh axis runs over, the one named last changes fastest.
Arguments:
- query_rows: bfloat16 [1024, 1024], P(('grp', 'sp'), 'tp'), parts along dimension 0, may hold values from -12 to 12
- key_rows: bfloat16 [1024, 1024], P(('grp', 'sp'), 'tp'), parts along dimension 0, may hold values from -9 to 9
- value_rows: bfloat16 [1024, 1024], P(('grp', 'sp'), 'tp'), parts along dimension 0, may hold values from -6 to 6
- key_logit: bfloat16 [1024, 8], P(('grp', 'sp'), 'tp'), parts along dimension 0, as said below
- residual: bfloat16 [1024, 2048], P(('grp', 'sp')), parts along dimension 0, may hold values from -6 to 6
- out_weight: bfloat16 [1024, 2048], P('tp'), may hold values from -0.1875 to 0.1875
- mix_gain: float32 [2048], replicated, may hold values from 0.1 to 1.9
- ffn_gain: float32 [2048], replicated, may hold values from 0.1 to 1.9
- out_gain: float32 [2048], replicated, may hold values from 0.1 to 1.9
- gate_weight: bfloat16 [2048, 5120], P('sp', 'tp'), may hold values from -0.125 to 0.125
- up_weight: bfloat16 [2048, 5120], P('sp', 'tp'), may hold values from -0.125 to 0.125
- down_weight: bfloat16 [2048, 5120], P('sp', 'tp'), may hold values from -0.078125 to 0.078125
Outputs:
- layer_out: bfloat16 [1024, 2048], P(('grp', 'sp')), parts along dimension 0
There are 2 independent parts, one for each index of `grp`. A program takes and returns all parts, laid end to end along the dimension named above; an argument that names none is the same for every part. Nothing has to cross between parts.
Inputs may be any that keep to these rules, and one draw needn't show every extreme that they name: `key_logit`: log-odds offsets of the keys, all negative.
All inputs are finite; a program needn't handle non-finite values.
Results may differ from a plain program's by a relative error of at most 0.018.
Values may be sent and summed in bfloat16 or wider, within the bound.
No kernel may reach another device: no remote copies, remote signals or barrier semaphores. Data moves between devices by JAX's collectives and lax.ppermute only.
A program may use at most 64 MiB of HBM per device.

v0:
```python
import jax
import jax.numpy as jnp
from jax import lax
from jax.sharding import PartitionSpec as P

epsilon = 1e-06


def normalize(payload_table):
    return payload_table * lax.rsqrt(
        jnp.mean(payload_table * payload_table, axis=-1, keepdims=True) + epsilon
    )


def shards(
    query_rows,
    key_rows,
    value_rows,
    key_logit,
    residual,
    out_weight,
    mix_gain,
    ffn_gain,
    out_gain,
    gate_weight,
    up_weight,
    down_weight,
):
    tok_rows = query_rows.shape[0]
    head_count = key_logit.shape[1]
    head_width = query_rows.shape[1] // head_count
    block_count = lax.axis_size("sp")
    own_block = lax.axis_index("sp")
    queries = query_rows.reshape(tok_rows, head_count, head_width).transpose(1, 0, 2)
    score_scale = head_width ** (-0.5)
    query_pos = own_block * tok_rows + jnp.arange(tok_rows, dtype=jnp.int32)[:, None]

    def group_terms(key_part, value_part, logit_part, first_block):
        span_rows = key_part.shape[0]
        shard_count = span_rows // tok_rows

        def compute(unused):
            scores = (
                jnp.einsum(
                    "hqd,khd->hqk",
                    queries,
                    key_part.reshape(span_rows, head_count, head_width),
                    preferred_element_type=jnp.float32,
                )
                * score_scale
            )
            scores = scores + jnp.transpose(logit_part.astype(jnp.float32))[:, None, :]
            key_pos = first_block * tok_rows + jnp.arange(span_rows, dtype=jnp.int32)[None, :]
            causal = (key_pos < query_pos).reshape(tok_rows, shard_count, tok_rows)
            scores = scores.reshape(head_count, tok_rows, shard_count, tok_rows)
            keep_log = jnp.where(causal, jax.nn.log_sigmoid(-scores), 0.0)
            within = lax.cumsum(keep_log, axis=3, reverse=True) - keep_log
            sticks = jnp.where(causal, jnp.exp(jax.nn.log_sigmoid(scores) + within), 0.0).astype(
                jnp.bfloat16
            )
            partials = jnp.einsum(
                "hqgk,gkhd->ghqd",
                sticks,
                value_part.reshape(shard_count, tok_rows, head_count, head_width),
                preferred_element_type=jnp.float32,
            )
            return (jnp.sum(keep_log, axis=3), partials)

        def skipped(unused):
            return (
                jnp.zeros((head_count, tok_rows, shard_count), jnp.float32),
                jnp.zeros((shard_count, head_count, tok_rows, head_width), jnp.float32),
            )

        return lax.cond(first_block <= own_block, compute, skipped, 0)

    initial = (
        jnp.zeros((head_count, tok_rows, block_count), jnp.float32),
        jnp.zeros((block_count, head_count, tok_rows, head_width), jnp.float32),
    )
    tables = initial
    key_part = lax.all_gather(key_rows, "sp", axis=0, tiled=True)
    value_part = lax.all_gather(value_rows, "sp", axis=0, tiled=True)
    logit_part = lax.all_gather(key_logit, "sp", axis=0, tiled=True)
    shard_count = key_part.shape[0] // tok_rows
    group_size = 2
    span_rows = group_size * tok_rows

    def one_group(carried, group_index):
        offset = group_index * span_rows
        first_block = group_index * group_size
        totals, partials = group_terms(
            lax.dynamic_slice_in_dim(key_part, offset, span_rows, 0),
            lax.dynamic_slice_in_dim(value_part, offset, span_rows, 0),
            lax.dynamic_slice_in_dim(logit_part, offset, span_rows, 0),
            first_block,
        )
        carried = (
            lax.dynamic_update_slice(carried[0], totals, (0, 0, first_block)),
            lax.dynamic_update_slice(carried[1], partials, (first_block, 0, 0, 0)),
        )
        return (carried, None)

    tables, unused = lax.scan(
        one_group, tables, jnp.arange(shard_count // group_size, dtype=jnp.int32)
    )
    totals, partials = tables
    suffix = lax.cumsum(totals, axis=2, reverse=True) - totals
    attended = jnp.einsum(
        "hqb,bhqd->qhd", jnp.exp(suffix), partials, precision=lax.Precision.HIGHEST
    )
    attended = attended.reshape(tok_rows, head_count * head_width).astype(jnp.bfloat16)
    head_part = jnp.dot(attended, out_weight, preferred_element_type=jnp.float32)
    mixed_rows = lax.psum(head_part.astype(jnp.bfloat16), "tp")
    middle = (
        residual.astype(jnp.float32) + mix_gain * normalize(mixed_rows.astype(jnp.float32))
    ).astype(jnp.bfloat16)
    normed = (ffn_gain * normalize(middle.astype(jnp.float32))).astype(jnp.bfloat16)
    gate_act = jnp.dot(
        normed,
        lax.all_gather(gate_weight, "sp", axis=0, tiled=True),
        preferred_element_type=jnp.float32,
    )
    up_act = jnp.dot(
        normed,
        lax.all_gather(up_weight, "sp", axis=0, tiled=True),
        preferred_element_type=jnp.float32,
    )
    hidden = (jax.nn.silu(gate_act) * up_act).astype(jnp.bfloat16)
    unit_part = lax.dot_general(
        hidden,
        lax.all_gather(down_weight, "sp", axis=0, tiled=True),
        (((1,), (1,)), ((), ())),
        preferred_element_type=jnp.float32,
    )
    ffn_out = lax.psum(unit_part.astype(jnp.bfloat16), "tp")
    return (middle.astype(jnp.float32) + out_gain * normalize(ffn_out.astype(jnp.float32))).astype(
        jnp.bfloat16
    )


def solution(mesh):
    placed = (
        P(("grp", "sp"), "tp"),
        P(("grp", "sp"), "tp"),
        P(("grp", "sp"), "tp"),
        P(("grp", "sp"), "tp"),
        P(("grp", "sp"), None),
        P("tp", None),
        P(),
        P(),
        P(),
        P("sp", "tp"),
        P("sp", "tp"),
        P("sp", "tp"),
    )
    return jax.shard_map(
        shards, mesh=mesh, in_specs=placed, out_specs=P(("grp", "sp"), None), check_vma=False
    )
```

profile of v0, /device:TPU:0, one launch (start us, length us, event | category | flops | bytes accessed | tf_op | source)
XLA Modules:
  0.0 408.5 jit_solution(9131922966451456633)
XLA Ops:
  7.4 1.0 copy.41
  8.4 14.5 %all_gather.18 = bf16[512,256]{0,1:T(8,128)(2,1)S(1)} all-gather(bf16[128,256]{0,1:T(8,128)(2,1)S(1)} %copy.41), channel_id=1, replica_groups=mesh['grp'=2,'sp'=4,'tp'=4] {'sp'}, dimensions={0}, use_global_device_ids=true | all-gather | bytes 327680 | tf_op jit(solution)/shard_map/all_gather | solution.py:82
  22.9 14.6 %all_gather.20 = bf16[512,256]{1,0:T(8,128)(2,1)S(1)} all-gather(bf16[128,256]{1,0:T(8,128)(2,1)} %param.18), channel_id=1, replica_groups=mesh['grp'=2,'sp'=4,'tp'=4] {'sp'}, dimensions={0}, use_global_device_ids=true | all-gather | bytes 327680 | tf_op jit(solution)/shard_map/all_gather | solution.py:83
  37.5 0.9 copy.42
  38.6 10.0 %all_gather.19 = bf16[512,2]{0,1:T(2,128)(2,1)S(1)} all-gather(bf16[128,2]{0,1:T(2,128)(2,1)} %param.19), channel_id=1, replica_groups=mesh['grp'=2,'sp'=4,'tp'=4] {'sp'}, dimensions={0}, use_global_device_ids=true | all-gather | bytes 2560 | tf_op jit(solution)/shard_map/all_gather | solution.py:84
  48.7 8.5 %while.13 = (s32[]{:T(128)}, f32[2,128,4]{1,2,0:T(4,128)S(1)}, f32[4,2,128,128]{3,0,1,2:T(4,128)S(1)}, s32[2]{0:T(128)S(1)}, s32[]{:T(128)}, /*index=5*/bf16[512...) while((s32[]{:T(128)}, f32[2,128,4]{1,2,0:T(4,128)S(1)}, ...), condition=%wide.region_5.6_spmd.clone, body=%wide.region_0.5_spmd.clone.sunk | while | flops 43418504 | bytes 4373875 | solution.py:104
  48.7 0.6 dynamic_slice.39
  49.9 5.3 %conditional.3 = (f32[2,128,2]{1,2,0:T(2,128)S(1)}, f32[2,2,128,128]{3,2,1,0:T(8,128)S(1)}) conditional(s32[]{:T(128)} %convert_element_type.116, () %tuple.48, (s32[]{:T(128)}, s32[]{:T(128)}, s32[]{:T(128)}, bf16[512,256]{0,1:T(8,128)(2,1)S(1)}, bf16[2,128,128]{2,1,0:T(8,128)(2,1)S(1)}, /*index=5*/bf16[512,2]{0,1:T(2,128)(2,1)S(1)}, ...), branch_computations={%region_1.1_spmd, %region_2.4_spmd} | conditional | flops 43418500 | bytes 3844702 | solution.py:75
  50.6 0.2 fusion.2
  51.1 0.8 fusion.35
  51.9 2.2 fusion.38
  54.0 0.9 select_convert_fusion
  55.0 0.2 fusion.8
  55.2 0.3 copy_dynamic-update-slice_fusion.2
  55.6 0.6 dynamic_slice.39
  56.9 0.3 copy_dynamic-update-slice_fusion.2
  57.5 1.8 fusion.39
  59.3 1.1 convolution_convert_fusion.1
  60.5 0.5 all-gather.4.cloned.1.call-update
  61.1 0.5 all-gather.6.cloned.1.call-update
  61.7 0.5 all-gather.8.cloned.1.call-update
  62.2 34.5 %all-reduce.3.cloned.1.call-done = bf16[128,2048]{1,0:T(8,128)(2,1)} async-done(((bf16[128,2048]{1,0:T(8,128)(2,1)}), bf16[128,2048]{1,0:T(8,128)(2,1)}) %all-reduce.3.cloned.1.call-update) | async-done | bytes 524304 | tf_op jit(solution)/shard_map/psum | solution.py:114
  96.8 1.2 fusion.12
  98.0 1.5 fusion.18
  99.5 63.6 %all-gather.4.cloned.1.call-done = bf16[2048,1280]{1,0:T(8,128)(2,1)} async-done(((bf16[512,1280]{1,0:T(8,128)(2,1)}), bf16[2048,1280]{1,0:T(8,128)(2,1)}) %all-gather.4.cloned.1.call-update) | async-done | bytes 5242896 | tf_op jit(solution)/shard_map/all_gather | solution.py:121
  163.1 3.4 fusion.30
  166.5 94.3 %all-gather.6.cloned.1.call-done = bf16[2048,1280]{1,0:T(8,128)(2,1)} async-done(((bf16[512,1280]{1,0:T(8,128)(2,1)}), bf16[2048,1280]{1,0:T(8,128)(2,1)}) %all-gather.6.cloned.1.call-update) | async-done | bytes 5242896 | tf_op jit(solution)/shard_map/all_gather | solution.py:126
  260.8 97.7 %all-gather.8.cloned.1.call-done = bf16[2048,1280]{1,0:T(8,128)(2,1)} async-done(((bf16[512,1280]{1,0:T(8,128)(2,1)}), bf16[2048,1280]{1,0:T(8,128)(2,1)}) %all-gather.8.cloned.1.call-update) | async-done | bytes 5242896 | tf_op jit(solution)/shard_map/all_gather | solution.py:132
  358.5 7.2 %convolution_convert_fusion = bf16[128,2048]{1,0:T(8,128)(2,1)} fusion(bf16[2048,1280]{1,0:T(8,128)(2,1)} %all-gather.8.cloned.1.call-done, bf16[2048,1280]{1,0:T(8,128)(2,1)} %all-gather.6.cloned.1.call-done, f32[128,1280]{1,0:T(8,128)S(1)} %fusion.30, bf16[128,2048]{1,0:T(8,128)(2,1)S(1)} %get-tuple-element.241, f32[128]{0:T(128)S(1)} %add_rsqrt_fusion.1, ...), kind=kOutput, calls=%fused_computation.23 | convolution fusion | flops 1344471040 | bytes 12198400 | tf_op jit(solution)/shard_map/dot_general | solution.py:130
  365.7 31.9 %all-reduce.5.cloned.1.call-done = bf16[128,2048]{1,0:T(8,128)(2,1)} async-done(((bf16[128,2048]{1,0:T(8,128)(2,1)}), bf16[128,2048]{1,0:T(8,128)(2,1)}) %all-reduce.5.cloned.1.call-update) | async-done | bytes 524304 | tf_op jit(solution)/shard_map/psum | solution.py:136
  397.6 1.2 fusion.16
  398.9 2.1 fusion.21
  (42 shorter events, 1.1 us)
Async XLA Ops:
  7.4 51.9 %copy-start = (bf16[256,2048]{1,0:T(8,128)(2,1)S(1)}, bf16[256,2048]{1,0:T(8,128)(2,1)}, u32[]{:S(2)}) copy-start(bf16[256,2048]{1,0:T(8,128)(2,1)} %param.21) | copy-start | bytes 3145732
  7.4 89.4 %all-reduce.3.cloned.1.call-start = ((), (), s32[]{:S(2)}) async-start(), calls=%async_computation | async-start | bytes 1048576 | tf_op jit(solution)/shard_map/psum | solution.py:114
  57.2 40.8 %copy-start.1 = (bf16[128,2048]{1,0:T(8,128)(2,1)S(1)}, bf16[128,2048]{1,0:T(8,128)(2,1)}, u32[]{:S(2)}) copy-start(bf16[128,2048]{1,0:T(8,128)(2,1)} %param.20) | copy-start | bytes 1572868
  57.2 40.8 %copy-start.2 = (f32[2048]{0:T(1024)S(1)}, f32[2048]{0:T(1024)}, u32[]{:S(2)}) copy-start(f32[2048]{0:T(1024)} %param.22) | copy-start | bytes 24580
  57.2 105.8 %copy-start.3 = (f32[2048]{0:T(1024)S(1)}, f32[2048]{0:T(1024)}, u32[]{:S(2)}) copy-start(f32[2048]{0:T(1024)} %param.23) | copy-start | bytes 24580
  60.4 102.6 %all-gather.4.cloned.1.call-start = ((), (), s32[]{:S(2)}) async-start(), calls=%async_computation.1 | async-start | bytes 6553600 | tf_op jit(solution)/shard_map/all_gather | solution.py:121
  61.0 199.8 %all-gather.6.cloned.1.call-start = ((), (), s32[]{:S(2)}) async-start(), calls=%async_computation.2 | async-start | bytes 6553600 | tf_op jit(solution)/shard_map/all_gather | solution.py:126
  61.6 296.9 %all-gather.8.cloned.1.call-start = ((), (), s32[]{:S(2)}) async-start(), calls=%async_computation.3 | async-start | bytes 6553600 | tf_op jit(solution)/shard_map/all_gather | solution.py:132
  62.2 335.4 %all-reduce.5.cloned.1.call-start = ((), (), s32[]{:S(2)}) async-start(), calls=%async_computation.4 | async-start | bytes 1048576 | tf_op jit(solution)/shard_map/psum | solution.py:136
  166.5 232.4 %copy-start.4 = (f32[2048]{0:T(1024)S(1)}, f32[2048]{0:T(1024)}, u32[]{:S(2)}) copy-start(f32[2048]{0:T(1024)} %param.24) | copy-start | bytes 24580
Sparse Core Ops, SparseCore 0:
  60.6 36.1 all-reduce.2
  365.9 31.7 all-reduce.4
Sparse Core Ops, SparseCore 1:
  62.5 100.5 all-gather.3
  164.5 96.2 all-gather.5
  262.2 96.2 all-gather.7
where the time goes:
time: 409 us
  waiting for transfers between devices  324 us (79%)
  blocking collectives  39.1 us (10%)
  between operations  15.1 us (4%)
  matrix products  14 us (3%)
  other arithmetic  10.2 us (2%)
  local copies, waits for them, and re-layouts  4.28 us (1%)
    all_gather x1, waiting for transfers between devices, shards(): lax.all_gather(down_weight, 'sp', axis=0, tiled=True)  97.7 us
    all_gather x1, waiting for transfers between devices, shards(): lax.all_gather(up_weight, 'sp', axis=0, tiled=True)  94.3 us
    all_gather x1, waiting for transfers between devices, shards(): lax.all_gather(gate_weight, 'sp', axis=0, tiled=True)  63.6 us
    psum x1, waiting for transfers between devices, shards(): mixed_rows = lax.psum(head_part.astype(jnp.bfloat16), 'tp')  34.5 us
    psum x1, waiting for transfers between devices, shards(): ffn_out = lax.psum(unit_part.astype(jnp.bfloat16), 'tp')  31.9 us
    all_gather x1, blocking collectives, shards(): value_part = lax.all_gather(value_rows, 'sp', axis=0, tiled=True)  14.6 us
    all_gather x1, blocking collectives, shards(): key_part = lax.all_gather(key_rows, 'sp', axis=0, tiled=True)  14.5 us
    all_gather x1, blocking collectives, shards(): logit_part = lax.all_gather(key_logit, 'sp', axis=0, tiled=True)  10 us
  transfers between devices with their start and end apart: 5, of which 5 were waited for; matrix products, arithmetic and copies ran while one was open for 1% of the time, Pallas kernels for 0%

commit v1 on v0

--- a/solution.py
+++ b/solution.py
@@ -1,9 +1,17 @@
+import functools
 import jax
 import jax.numpy as jnp
 from jax import lax
 from jax.sharding import PartitionSpec as P
 
 epsilon = 1e-06
+
+
+def rows_apply(xx, along_axis):
+    return jax.lax.all_gather(xx, along_axis).sum(axis=0)
+
+
+shape_case_over_axis = functools.partial(rows_apply, along_axis="tp")
 
 
 def normalize(payload_table):
@@ -111,7 +119,7 @@
     )
     attended = attended.reshape(tok_rows, head_count * head_width).astype(jnp.bfloat16)
     head_part = jnp.dot(attended, out_weight, preferred_element_type=jnp.float32)
-    mixed_rows = lax.psum(head_part.astype(jnp.bfloat16), "tp")
+    mixed_rows = shape_case_over_axis(head_part.astype(jnp.bfloat16))
     middle = (
         residual.astype(jnp.float32) + mix_gain * normalize(mixed_rows.astype(jnp.float32))
     ).astype(jnp.bfloat16)

time: 409 us -> 430 us (1.051)
  waiting for transfers between devices: 324 us -> 346 us
    psum x1 -> x0, waiting for transfers between devices: 34.5 us -> none  [shards(): mixed_rows = lax.psum(head_part.astype(jnp.bfloat16), 'tp')]
    all_gather x1, waiting for transfers between devices: 63.6 us -> 97 us  [shards(): lax.all_gather(gate_weight, 'sp', axis=0, tiled=True)]
    all_gather x0 -> x1, waiting for transfers between devices: none -> 23.1 us  [rows_apply(): return jax.lax.all_gather(xx, along_axis).sum(axis=0)]
where the time goes in v1:
time: 430 us; the launch traced here: 429 us
  waiting for transfers between devices  346 us (80%)
  blocking collectives  39.1 us (9%)
  matrix products  14 us (3%)
  between operations  13.3 us (3%)
  other arithmetic  10.1 us (2%)
    all_gather x1, waiting for transfers between devices, shards(): lax.all_gather(up_weight, 'sp', axis=0, tiled=True)  97.8 us
    all_gather x1, waiting for transfers between devices, shards(): lax.all_gather(gate_weight, 'sp', axis=0, tiled=True)  97 us
    all_gather x1, waiting for transfers between devices, shards(): lax.all_gather(down_weight, 'sp', axis=0, tiled=True)  94.6 us
    psum x1, waiting for transfers between devices, shards(): ffn_out = lax.psum(unit_part.astype(jnp.bfloat16), 'tp')  31.9 us
    all_gather x1, waiting for transfers between devices, rows_apply(): return jax.lax.all_gather(xx, along_axis).sum(axis=0)  23.1 us
    all_gather x1, blocking collectives, shards(): value_part = lax.all_gather(value_rows, 'sp', axis=0, tiled=True)  14.6 us
    all_gather x1, blocking collectives, shards(): key_part = lax.all_gather(key_rows, 'sp', axis=0, tiled=True)  14.5 us
    all_gather x1, blocking collectives, shards(): logit_part = lax.all_gather(key_logit, 'sp', axis=0, tiled=True)  10 us
  transfers between devices with their start and end apart: 5, of which 5 were waited for; matrix products, arithmetic and copies ran while one was open for 1% of the time, Pallas kernels for 0%

profile of v1, /device:TPU:0, one launch (start us, length us, event | category | flops | bytes accessed | tf_op | source)
XLA Modules:
  0.0 429.4 jit_solution(2671783025213710686)
XLA Ops:
  6.5 1.0 copy.41
  7.6 14.5 %all_gather.24 = bf16[512,256]{0,1:T(8,128)(2,1)S(1)} all-gather(bf16[128,256]{0,1:T(8,128)(2,1)S(1)} %copy.41), channel_id=1, replica_groups=mesh['grp'=2,'sp'=4,'tp'=4] {'sp'}, dimensions={0}, use_global_device_ids=true | all-gather | bytes 327680 | tf_op jit(solution)/shard_map/all_gather | solution.py:90
  22.1 14.6 %all_gather.26 = bf16[512,256]{1,0:T(8,128)(2,1)S(1)} all-gather(bf16[128,256]{1,0:T(8,128)(2,1)} %param.18), channel_id=1, replica_groups=mesh['grp'=2,'sp'=4,'tp'=4] {'sp'}, dimensions={0}, use_global_device_ids=true | all-gather | bytes 327680 | tf_op jit(solution)/shard_map/all_gather | solution.py:91
  36.6 0.9 copy.42
  37.7 10.0 %all_gather.25 = bf16[512,2]{0,1:T(2,128)(2,1)S(1)} all-gather(bf16[128,2]{0,1:T(2,128)(2,1)} %param.19), channel_id=1, replica_groups=mesh['grp'=2,'sp'=4,'tp'=4] {'sp'}, dimensions={0}, use_global_device_ids=true | all-gather | bytes 2560 | tf_op jit(solution)/shard_map/all_gather | solution.py:92
  47.8 8.5 %while.13 = (s32[]{:T(128)}, f32[2,128,4]{1,2,0:T(4,128)S(1)}, f32[4,2,128,128]{3,0,1,2:T(4,128)S(1)}, s32[2]{0:T(128)S(1)}, s32[]{:T(128)}, /*index=5*/bf16[512...) while((s32[]{:T(128)}, f32[2,128,4]{1,2,0:T(4,128)S(1)}, ...), condition=%wide.region_5.6_spmd.clone, body=%wide.region_0.5_spmd.clone.sunk | while | flops 43418504 | bytes 4373875 | solution.py:112
  47.9 0.6 dynamic_slice.39
  49.1 5.3 %conditional.3 = (f32[2,128,2]{1,2,0:T(2,128)S(1)}, f32[2,2,128,128]{3,2,1,0:T(8,128)S(1)}) conditional(s32[]{:T(128)} %convert_element_type.118, () %tuple.48, (s32[]{:T(128)}, s32[]{:T(128)}, s32[]{:T(128)}, bf16[512,256]{0,1:T(8,128)(2,1)S(1)}, bf16[2,128,128]{2,1,0:T(8,128)(2,1)S(1)}, /*index=5*/bf16[512,2]{0,1:T(2,128)(2,1)S(1)}, ...), branch_computations={%region_1.1_spmd, %region_2.4_spmd} | conditional | flops 43418500 | bytes 3844702 | solution.py:83
  49.8 0.2 fusion.2
  50.3 0.8 fusion.35
  51.0 2.2 fusion.38
  53.2 0.9 select_convert_fusion
  54.2 0.2 fusion.8
  54.4 0.3 copy_dynamic-update-slice_fusion.2
  54.7 0.6 dynamic_slice.39
  56.0 0.3 copy_dynamic-update-slice_fusion.2
  56.6 1.8 fusion.39
  58.5 1.1 convolution_convert_fusion.1
  59.7 0.7 all-gather.6.cloned.1.call-update
  60.4 0.7 all-gather.10.cloned.1.call-update
  61.1 0.5 all-gather.8.cloned.1.call-update
  61.9 23.1 %all-gather.12.cloned.1.call-done = bf16[512,2048]{1,0:T(8,128)(2,1)} async-done(((bf16[128,2048]{1,0:T(8,128)(2,1)}), bf16[512,2048]{1,0:T(8,128)(2,1)}) %all-gather.12.cloned.1.call-update) | async-done | bytes 2097168 | tf_op jit(solution)/shard_map/all_gather | solution.py:11
  85.0 2.0 reduce_sum.52
  87.2 0.4 fusion.18
  87.6 97.0 %all-gather.6.cloned.1.call-done = bf16[2048,1280]{1,0:T(8,128)(2,1)} async-done(((bf16[512,1280]{1,0:T(8,128)(2,1)}), bf16[2048,1280]{1,0:T(8,128)(2,1)}) %all-gather.6.cloned.1.call-update) | async-done | bytes 5242896 | tf_op jit(solution)/shard_map/all_gather | solution.py:129
  184.6 3.4 fusion.30
  188.0 94.6 %all-gather.10.cloned.1.call-done = bf16[2048,1280]{1,0:T(8,128)(2,1)} async-done(((bf16[512,1280]{1,0:T(8,128)(2,1)}), bf16[2048,1280]{1,0:T(8,128)(2,1)}) %all-gather.10.cloned.1.call-update) | async-done | bytes 5242896 | tf_op jit(solution)/shard_map/all_gather | solution.py:140
  282.6 97.8 %all-gather.8.cloned.1.call-done = bf16[2048,1280]{1,0:T(8,128)(2,1)} async-done(((bf16[512,1280]{1,0:T(8,128)(2,1)}), bf16[2048,1280]{1,0:T(8,128)(2,1)}) %all-gather.8.cloned.1.call-update) | async-done | bytes 5242896 | tf_op jit(solution)/shard_map/all_gather | solution.py:134
  380.4 7.2 %convolution_convert_fusion = bf16[128,2048]{1,0:T(8,128)(2,1)} fusion(bf16[2048,1280]{1,0:T(8,128)(2,1)} %all-gather.10.cloned.1.call-done, bf16[2048,1280]{1,0:T(8,128)(2,1)} %all-gather.8.cloned.1.call-done, f32[128,1280]{1,0:T(8,128)S(1)} %fusion.30, bf16[128,2048]{1,0:T(8,128)(2,1)S(1)} %get-tuple-element.241, f32[128]{0:T(128)S(1)} %add_rsqrt_fusion.1, ...), kind=kOutput, calls=%fused_computation.23 | convolution fusion | flops 1344471040 | bytes 12198400 | tf_op jit(solution)/shard_map/dot_general | solution.py:138
  387.7 31.9 %all-reduce.2.cloned.1.call-done = bf16[128,2048]{1,0:T(8,128)(2,1)} async-done(((bf16[128,2048]{1,0:T(8,128)(2,1)}), bf16[128,2048]{1,0:T(8,128)(2,1)}) %all-reduce.2.cloned.1.call-update) | async-done | bytes 524304 | tf_op jit(solution)/shard_map/psum | solution.py:144
  419.6 1.2 fusion.16
  420.8 2.1 fusion.21
  (43 shorter events, 1.5 us)
Async XLA Ops:
  6.5 51.9 %copy-start = (bf16[256,2048]{1,0:T(8,128)(2,1)S(1)}, bf16[256,2048]{1,0:T(8,128)(2,1)}, u32[]{:S(2)}) copy-start(bf16[256,2048]{1,0:T(8,128)(2,1)} %param.21) | copy-start | bytes 3145732
  6.5 78.4 %all-gather.12.cloned.1.call-start = ((), (), s32[]{:S(2)}) async-start(), calls=%async_computation.4 | async-start | bytes 2621440 | tf_op jit(solution)/shard_map/all_gather | solution.py:11
  56.6 30.6 %copy-start.1 = (bf16[128,2048]{1,0:T(8,128)(2,1)S(1)}, bf16[128,2048]{1,0:T(8,128)(2,1)}, u32[]{:S(2)}) copy-start(bf16[128,2048]{1,0:T(8,128)(2,1)} %param.20) | copy-start | bytes 1572868
  56.6 30.6 %copy-start.2 = (f32[2048]{0:T(1024)S(1)}, f32[2048]{0:T(1024)}, u32[]{:S(2)}) copy-start(f32[2048]{0:T(1024)} %param.22) | copy-start | bytes 24580
  58.5 126.1 %copy-start.3 = (f32[2048]{0:T(1024)S(1)}, f32[2048]{0:T(1024)}, u32[]{:S(2)}) copy-start(f32[2048]{0:T(1024)} %param.23) | copy-start | bytes 24580
  59.6 125.0 %all-gather.6.cloned.1.call-start = ((), (), s32[]{:S(2)}) async-start(), calls=%async_computation | async-start | bytes 6553600 | tf_op jit(solution)/shard_map/all_gather | solution.py:129
  60.4 222.2 %all-gather.10.cloned.1.call-start = ((), (), s32[]{:S(2)}) async-start(), calls=%async_computation.2 | async-start | bytes 6553600 | tf_op jit(solution)/shard_map/all_gather | solution.py:140
  61.1 319.3 %all-gather.8.cloned.1.call-start = ((), (), s32[]{:S(2)}) async-start(), calls=%async_computation.1 | async-start | bytes 6553600 | tf_op jit(solution)/shard_map/all_gather | solution.py:134
  61.7 357.9 %all-reduce.2.cloned.1.call-start = ((), (), s32[]{:S(2)}) async-start(), calls=%async_computation.3 | async-start | bytes 1048576 | tf_op jit(solution)/shard_map/psum | solution.py:144
  188.0 232.8 %copy-start.4 = (f32[2048]{0:T(1024)S(1)}, f32[2048]{0:T(1024)}, u32[]{:S(2)}) copy-start(f32[2048]{0:T(1024)} %param.24) | copy-start | bytes 24580
Sparse Core Ops, SparseCore 0:
  59.7 25.1 all-gather.11
  86.5 98.0 all-gather.5
  186.2 96.3 all-gather.9
  284.0 96.3 all-gather.7
  387.8 31.7 all-reduce.1
